TPU v7x, 32 devices: a whole 2x2x4 slice. The times are simulated.
32 devices in a mesh: fs: 8 (over z, y), tp: 4 (over x, core).
Axes of the slice: x: 2, y: 2, z: 4, core: 2. Of those that a mesh axis runs over, the one named last changes fastest.
Arguments:
- tokens: bfloat16 [6144, 2048], P('fs'), may hold values from -6 to 6
- routes: int32 [6144, 2], P('fs'), may hold values from 0 to 7, all different within a row; in each aligned block of 768 rows (0 to 767, 768 to 1535, ...) at most 216 rows name the same one
- route_weight: float32 [6144, 2], P('fs'), may hold values from 0.2 to 1
- norm_gain: float32 [2048], P('fs'), may hold values from 0.1 to 1.9
- gate_master: float32 [8, 2048, 4096], P(None, 'fs', 'tp'), may hold values from -0.125 to 0.125
- up_master: float32 [8, 2048, 4096], P(None, 'fs', 'tp'), may hold values from -0.125 to 0.125
- down_master: float32 [8, 4096, 2048], P(None, 'fs', 'tp'), may hold values from -0.09375 to 0.09375
Outputs:
- gate_serve: bfloat16 [8, 2048, 4096], P('fs', None, 'tp')
- up_serve: bfloat16 [8, 2048, 4096], P('fs', None, 'tp')
- down_serve: bfloat16 [8, 4096, 2048], P('fs', 'tp')
- layer_out: bfloat16 [6144, 2048], P('fs', 'tp')
Inputs may be any that keep to these rules, and one draw needn't show every extreme that they name: `routes`: each row names two different experts; among the 768 rows of one index of fs no expert is named by more than 216 rows, a bound that some block reaches.
All inputs are finite; a program needn't handle non-finite values.
Results may differ from a plain program's by a relative error of at most 0.015.
Values may be sent and summed in bfloat16 or wider, within the bound.
A program may use at most 192 MiB of HBM per device.

v0:
```python
import functools

import jax
import jax.numpy as jnp
from jax import lax
from jax.experimental import pallas as pl
from jax.experimental.pallas import tpu as pltpu
from jax.sharding import PartitionSpec as P

CAP = 216
ROWS = 224
DEPTH = 256
LANES = 128
STAGES = 3
MESH = pl.DeviceIdType.MESH
F32, BF16 = jnp.float32, jnp.bfloat16


def aligned(value, step=LANES):
    return pl.multiple_of(value, step)


def kernel(
    n_fs, n_tp, routes_in, routes_across_in, weight_in, gain_in, tokens_in, gate_in, up_in, down_in,
    gate_out, up_out, down_out, layer_out,
    gate_send, gate_recv, up_send, up_recv, down_send, down_recv, stage, down_stage,
    tokens, normed, outgoing, incoming, hidden, far, far_recv, near, across_recv,
    back_send, back_recv, result, gain_row, gain, routes, routes_across, weight, slot_across, slot, share,
    load_sem, down_load_sem, small_sem, gate_ss, gate_rs, up_ss, up_rs, token_ss, token_rs,
    down_ss, down_rs, line_ss, line_rs, pair_ss, pair_rs, far_ss, far_rs, across_ss, across_rs,
    back_ss, back_rs, gate_os, up_os, down_os, out_sem,
):
    f, t = lax.axis_index("fs"), lax.axis_index("tp")
    core, x = t % 2, t // 2
    chips = n_tp // 2
    ratio = n_fs // n_tp
    rows, units = gate_send.shape[1:]
    part = down_stage.shape[1]
    columns = down_stage.shape[2]
    chunks = columns // LANES
    count = tokens.shape[0]
    half = n_fs // 2

    def remote(src, dst, ss, rs, fs, tp):
        return pltpu.make_async_remote_copy(
            src_ref=src, dst_ref=dst, send_sem=ss, recv_sem=rs,
            device_id={"fs": fs, "tp": tp}, device_id_type=MESH,
        )

    def each(n, action):
        def step(i, carry):
            action(i)
            return carry

        lax.fori_loop(0, n, step, 0)

    def offset(i):
        return jnp.where(i < half, i + half, jnp.where(i == n_fs - 1, 0, i - half + 1))

    small = [
        pltpu.make_async_copy(gain_in, gain_row, small_sem.at[0]),
        pltpu.make_async_copy(routes_in, routes, small_sem.at[1]),
        pltpu.make_async_copy(routes_across_in, routes_across, small_sem.at[2]),
        pltpu.make_async_copy(weight_in, weight, small_sem.at[3]),
        pltpu.make_async_copy(tokens_in, tokens, small_sem.at[4]),
    ]
    small[0].start()

    def load(source, i):
        return pltpu.make_async_copy(
            source.at[jnp.bitwise_xor(f, offset(i))], stage.at[i % STAGES], load_sem.at[i % STAGES]
        )

    for i in range(STAGES):
        load(gate_in, i).start()
    for copy in small[1:]:
        copy.start()

    barrier = pltpu.get_barrier_semaphore()
    total = n_fs * n_tp
    me = f * n_tp + t

    def greet(i):
        other = (me + i + 1) % total
        pl.semaphore_signal(
            barrier, inc=1, device_id={"fs": other // n_tp, "tp": other % n_tp}, device_id_type=MESH
        )

    each(total - 1, greet)

    back_recv[:, :, CAP:, :] = jnp.zeros((chunks, n_fs, DEPTH - CAP, LANES), BF16)

    small[0].wait()
    same = lax.broadcasted_iota(jnp.int32, (rows, rows), 0) == lax.broadcasted_iota(jnp.int32, (rows, rows), 1)
    column = jnp.sum(jnp.where(same, gain_row[...], 0.0), axis=1, keepdims=True)
    gain[...] = jnp.broadcast_to(column, (rows, LANES))

    def weight_copy(send, recv, ss, rs, e, owner):
        return remote(
            send.at[e], recv.at[pl.ds(aligned(owner * rows), rows)], ss.at[e], rs.at[owner], e, t
        )

    def scaled(block):
        scale = gain[...]
        return jnp.concatenate(
            [(block[:, k : k + LANES] * scale).astype(BF16) for k in range(0, units, LANES)], axis=1
        )

    def send_weights(source, following, send, recv, ss, rs):
        def step(i):
            e = jnp.bitwise_xor(f, offset(i))
            load(source, i).wait()
            cast = scaled(stage[i % STAGES])

            @pl.when(i < n_fs - 1)
            def _():
                send[e] = cast

            @pl.when(i == n_fs - 1)
            def _():
                recv[pl.ds(aligned(f * rows), rows), :] = cast

            @pl.when(i + STAGES < n_fs)
            def _():
                load(source, i + STAGES).start()

            if following is not None:

                @pl.when(i + STAGES >= n_fs)
                def _():
                    j = i + STAGES - n_fs
                    pltpu.make_async_copy(
                        following.at[jnp.bitwise_xor(f, offset(j))],
                        stage.at[i % STAGES],
                        load_sem.at[i % STAGES],
                    ).start()

            if ss is not None:

                @pl.when(i > 0)
                def _():
                    weight_copy(send, recv, ss, rs, jnp.bitwise_xor(f, offset(i - 1)), f).start()

        return step

    pl.semaphore_wait(barrier, total - 1)
    each(n_fs, send_weights(gate_in, None, gate_send, gate_recv, gate_ss, gate_rs))
    for i in range(STAGES):
        load(up_in, i).start()

    for copy in small[1:4]:
        copy.wait()
    row_id = lax.broadcasted_iota(jnp.int32, (count, count), 0)
    column_id = lax.broadcasted_iota(jnp.int32, (count, count), 1)
    expert_row = lax.broadcasted_iota(jnp.int32, (n_fs, count), 0)
    named = (expert_row == routes_across[0:1, :]) | (expert_row == routes_across[1:2, :])
    before = jnp.dot(
        jnp.where(named, 1.0, 0.0).astype(BF16),
        jnp.where(row_id < column_id, 1.0, 0.0).astype(BF16),
        preferred_element_type=F32,
    )
    slot_across[...] = jnp.where(named, before, -1.0)
    expert_lane = lax.broadcasted_iota(jnp.int32, (count, LANES), 1)
    first, second = expert_lane == routes[:, 0:1], expert_lane == routes[:, 1:2]
    before = jnp.dot(
        jnp.where(column_id < row_id, 1.0, 0.0).astype(BF16),
        jnp.where(first | second, 1.0, 0.0).astype(BF16),
        preferred_element_type=F32,
    )
    slot[...] = jnp.where(first | second, before, -1.0)
    share[...] = jnp.where(first, weight[:, 0:1], 0.0) + jnp.where(second, weight[:, 1:2], 0.0)

    small[4].wait()
    strip = 96

    def norm(i):
        at = pl.ds(aligned(i * strip, strip), strip)
        values = tokens[at, :].astype(F32)
        scale = lax.rsqrt(jnp.mean(values * values, axis=1, keepdims=True) + 1e-06)
        mine = tokens[at, pl.ds(aligned(t * columns), columns)].astype(F32)
        normed[at, :] = (mine * scale).astype(BF16)

    each(count // strip, norm)

    def token_copy(e, owner):
        return remote(
            outgoing.at[e, pl.ds(0, CAP)],
            incoming.at[owner, pl.ds(0, CAP), pl.ds(aligned(t * columns), columns)],
            token_ss.at[e],
            token_rs.at[owner],
            e,
            t,
        )

    slot_id = lax.broadcasted_iota(jnp.int32, (ROWS, count), 0).astype(F32)

    def dispatch(i):
        e = jnp.bitwise_xor(f, offset(i))
        pick = jnp.where(slot_id == slot_across[pl.ds(e, 1), :], 1.0, 0.0).astype(BF16)
        picked = jnp.dot(pick, normed[...], preferred_element_type=F32).astype(BF16)

        @pl.when(i < n_fs - 1)
        def _():
            outgoing[e] = picked

        @pl.when(i == n_fs - 1)
        def _():
            incoming[f, :, pl.ds(aligned(t * columns), columns)] = picked

        @pl.when(i > 0)
        def _():
            token_copy(jnp.bitwise_xor(f, offset(i - 1)), f).start()

    each(n_fs, dispatch)

    each(n_fs, send_weights(up_in, None, up_send, up_recv, up_ss, up_rs))

    def down_load(i):
        return pltpu.make_async_copy(down_in.at[i], down_stage.at[i % 2], down_load_sem.at[i % 2])

    owner = f // ratio

    def place(tp):
        return aligned((tp % 2 * chips + tp // 2) * LANES)

    def down_copy(c, e, to, fs, tp):
        return remote(
            down_send.at[c, e],
            down_recv.at[c, pl.ds(aligned(fs % ratio * part), part), pl.ds(place(tp), LANES)],
            down_ss.at[c, e],
            down_rs.at[c, fs % ratio * n_tp + tp],
            e,
            to,
        )

    down_load(0).start()
    down_load(1).start()

    def down_cast(i):
        down_load(i).wait()
        for c in range(chunks):
            down_send[c, i] = down_stage[i % 2, :, c * LANES : (c + 1) * LANES].astype(BF16)

        @pl.when(i + 2 < n_fs)
        def _():
            down_load(i + 2).start()

    each(n_fs, down_cast)

    def send_down(c):
        def one(i):
            e = jnp.bitwise_xor(f, offset(i))
            mine = (e == f) & (owner == t)

            @pl.when(mine)
            def _():
                down_recv[c, pl.ds(aligned(f % ratio * part), part), pl.ds(place(t), LANES)] = down_send[c, e]

            @pl.when(jnp.logical_not(mine))
            def _():
                down_copy(c, e, owner, f, t).start()

        each(n_fs, one)

    def peers(action):
        each(n_fs - 1, lambda i: action(jnp.bitwise_xor(f, i + 1)))

    peers(lambda e: token_copy(e, e).wait_recv())

    def span(tp):
        return incoming.at[:, pl.ds(0, CAP), pl.ds(aligned(tp * columns), columns)]

    def line(d, chip):
        other = jnp.bitwise_xor(x, d)
        return remote(
            span(chip * 2 + core), span(chip * 2 + core), line_ss.at[d - 1], line_rs.at[d - 1], f, other * 2 + core
        )

    def pair(d, on):
        chip = jnp.bitwise_xor(x, d)
        return remote(
            span(chip * 2 + on), span(chip * 2 + on), pair_ss.at[d], pair_rs.at[d], f, x * 2 + 1 - core
        )

    for d in range(1, chips):
        line(d, x).start()
    pair(0, core).start()
    send_down(0)
    for d in range(1, chips):
        line(d, jnp.bitwise_xor(x, d)).wait_recv()
        pair(d, core).start()
    for d in range(chips):
        pair(d, 1 - core).wait_recv()

    peers(lambda e: weight_copy(gate_send, gate_recv, gate_ss, gate_rs, e, e).wait_recv())
    gate_store = pltpu.make_async_copy(gate_recv, gate_out, gate_os)
    gate_store.start()
    peers(lambda e: weight_copy(up_send, up_recv, up_ss, up_rs, e, e).wait_recv())
    up_store = pltpu.make_async_copy(up_recv, up_out, up_os)
    up_store.start()
    for c in range(1, chunks):
        send_down(c)

    tile = 256
    width = incoming.shape[2]
    group = 2

    def hidden_step(i):
        g, n = i // (units // tile), i % (units // tile)
        lanes = pl.ds(aligned(n * tile, tile), tile)
        at = pl.ds(g * group, group)
        received = incoming[at].reshape(group * ROWS, width)
        gate_pre = jnp.dot(received, gate_recv[:, lanes], preferred_element_type=F32)
        up_pre = jnp.dot(received, up_recv[:, lanes], preferred_element_type=F32)
        value = gate_pre / (1.0 + jnp.exp(-gate_pre)) * up_pre
        hidden[at, :, lanes] = value.astype(BF16).reshape(group, ROWS, tile)

    each(n_fs // group * (units // tile), hidden_step)

    def far_copy(c):
        return remote(far, far_recv.at[c], far_ss.at[c], far_rs.at[c], f, x * 2 + 1 - core)

    def across_copy(c, d):
        other = jnp.bitwise_xor(x, d)
        return remote(
            near.at[other], across_recv.at[c, d - 1], across_ss.at[c, d - 1], across_rs.at[c, d - 1],
            f, other * 2 + core,
        )

    def back_copy(c, e, owner):
        return remote(
            back_send.at[c, e, pl.ds(0, CAP)],
            back_recv.at[c, owner, pl.ds(0, CAP)],
            back_ss.at[c, e],
            back_rs.at[c, owner],
            e,
            t,
        )

    def send_back(c):
        peers(lambda e: back_copy(c, e, f).start())

    def down_store(c, tp):
        return pltpu.make_async_copy(
            down_recv.at[c, :, pl.ds(place(tp), LANES)],
            down_out.at[:, pl.ds(aligned(tp * columns + c * LANES), LANES)],
            down_os.at[c, tp],
        )

    def product(c, side, target):
        lanes = pl.ds(aligned(side * (chips * LANES)), chips * LANES)

        def step(g):
            at = pl.ds(g * group, group)
            value = jnp.dot(
                hidden[at].reshape(group * ROWS, units), down_recv[c, :, lanes], preferred_element_type=F32
            ).astype(BF16)
            for chip in range(chips):
                target[chip, at] = value[:, chip * LANES : (chip + 1) * LANES].reshape(group, ROWS, LANES)

        each(n_fs // group, step)

    def down_chunk(c):
        def arrival(i):
            fs, tp = owner_first + i // n_tp, i % n_tp

            @pl.when(jnp.logical_not((fs == f) & (tp == t)))
            def _():
                down_copy(c, f, t, fs, tp).wait_recv()

        owner_first = t * ratio
        each(ratio * n_tp, arrival)
        each(n_tp, lambda tp: down_store(c, tp).start())

        @pl.when(c == chunks - 1)
        def _():
            each(chunks - 1, send_back)

        product(c, 1 - core, far)
        far_copy(c).start()

        @pl.when(c > 0)
        def _():
            for d in range(1, chips):
                across_copy(c - 1, d).wait_send()

        product(c, core, near)
        far_copy(c).wait()
        for d in range(1, chips):
            other = jnp.bitwise_xor(x, d)

            def add(e):
                near[other, e] = (near[other, e].astype(F32) + far_recv[c, other, e].astype(F32)).astype(BF16)

            each(n_fs, add)
            across_copy(c, d).start()
        for d in range(1, chips):
            across_copy(c, d).wait_recv()

        def finish(e):
            value = near[x, e].astype(F32) + far_recv[c, x, e].astype(F32)
            for d in range(1, chips):
                value = value + across_recv[c, d - 1, e].astype(F32)
            back_send[c, e] = value.astype(BF16)

        each(n_fs, finish)
        back_recv[c, f, pl.ds(0, CAP), :] = back_send[c, f, pl.ds(0, CAP), :]

    each(chunks, down_chunk)
    send_back(chunks - 1)
    for d in range(1, chips):
        across_copy(chunks - 1, d).wait_send()

    lane_id = lax.broadcasted_iota(jnp.int32, (count, DEPTH), 1).astype(F32)

    def out_copy(c):
        return pltpu.make_async_copy(
            result.at[c], layer_out.at[:, pl.ds(aligned(c * LANES), LANES)], out_sem.at[c]
        )

    def combine(c):
        peers(lambda e: back_copy(c, e, e).wait_recv())
        value = jnp.zeros((count, LANES), F32)
        for e in range(n_fs):
            pick = jnp.where(lane_id == slot[:, e : e + 1], 1.0, 0.0).astype(BF16)
            value = value + share[:, e : e + 1] * jnp.dot(pick, back_recv[c, e], preferred_element_type=F32)
        result[c] = value.astype(BF16)
        out_copy(c).start()

    each(chunks, combine)

    peers(lambda e: weight_copy(gate_send, gate_recv, gate_ss, gate_rs, e, f).wait_send())
    peers(lambda e: weight_copy(up_send, up_recv, up_ss, up_rs, e, f).wait_send())
    peers(lambda e: token_copy(e, f).wait_send())
    for d in range(1, chips):
        line(d, x).wait_send()
    for d in range(chips):
        pair(d, core).wait_send()

    def drain(c):
        def one(e):
            @pl.when(jnp.logical_not((e == f) & (owner == t)))
            def _():
                down_copy(c, e, owner, f, t).wait_send()

        each(n_fs, one)
        each(n_tp, lambda tp: down_store(c, tp).wait())
        peers(lambda e: back_copy(c, e, f).wait_send())
        out_copy(c).wait()

    each(chunks, drain)
    gate_store.wait()
    up_store.wait()


def body(tokens, routes, route_weight, norm_gain, gate_master, up_master, down_master):
    n_fs, n_tp = lax.axis_size("fs"), lax.axis_size("tp")
    count, width = tokens.shape
    experts, rows, units = gate_master.shape
    part, columns = down_master.shape[1:]
    chips, chunks, ratio = n_tp // 2, columns // LANES, n_fs // n_tp
    assert experts == n_fs
    dma = pltpu.SemaphoreType.DMA
    lines = max(1, chips - 1)
    scratch = [
        pltpu.VMEM((n_fs, rows, units), BF16),
        pltpu.VMEM((n_fs * rows, units), BF16),
        pltpu.VMEM((n_fs, rows, units), BF16),
        pltpu.VMEM((n_fs * rows, units), BF16),
        pltpu.VMEM((chunks, n_fs, part, LANES), BF16),
        pltpu.VMEM((chunks, ratio * part, n_tp * LANES), BF16),
        pltpu.VMEM((STAGES, rows, units), F32),
        pltpu.VMEM((2, part, columns), F32),
        pltpu.VMEM((count, width), BF16),
        pltpu.VMEM((count, columns), BF16),
        pltpu.VMEM((n_fs, ROWS, columns), BF16),
        pltpu.VMEM((n_fs, ROWS, width), BF16),
        pltpu.VMEM((n_fs, ROWS, units), BF16),
        pltpu.VMEM((chips, n_fs, ROWS, LANES), BF16),
        pltpu.VMEM((chunks, chips, n_fs, ROWS, LANES), BF16),
        pltpu.VMEM((chips, n_fs, ROWS, LANES), BF16),
        pltpu.VMEM((chunks, lines, n_fs, ROWS, LANES), BF16),
        pltpu.VMEM((chunks, n_fs, ROWS, LANES), BF16),
        pltpu.VMEM((chunks, n_fs, DEPTH, LANES), BF16),
        pltpu.VMEM((chunks, count, LANES), BF16),
        pltpu.VMEM((1, rows), F32),
        pltpu.VMEM((rows, LANES), F32),
        pltpu.VMEM((count, 2), jnp.int32),
        pltpu.VMEM((2, count), jnp.int32),
        pltpu.VMEM((count, 2), F32),
        pltpu.VMEM((n_fs, count), F32),
        pltpu.VMEM((count, LANES), F32),
        pltpu.VMEM((count, LANES), F32),
        dma((STAGES,)), dma((2,)), dma((5,)),
        dma((n_fs,)), dma((n_fs,)), dma((n_fs,)), dma((n_fs,)), dma((n_fs,)), dma((n_fs,)),
        dma((chunks, n_fs)), dma((chunks, ratio * n_tp)),
        dma((lines,)), dma((lines,)), dma((chips,)), dma((chips,)),
        dma((chunks,)), dma((chunks,)), dma((chunks, lines)), dma((chunks, lines)),
        dma((chunks, n_fs)), dma((chunks, n_fs)),
        dma, dma, dma((chunks, n_tp)), dma((chunks,)),
    ]
    anywhere = pl.BlockSpec(memory_space=pl.ANY)
    return pl.pallas_call(
        functools.partial(kernel, n_fs, n_tp),
        out_shape=(
            jax.ShapeDtypeStruct((n_fs * rows, units), BF16),
            jax.ShapeDtypeStruct((n_fs * rows, units), BF16),
            jax.ShapeDtypeStruct((ratio * part, n_tp * columns), BF16),
            jax.ShapeDtypeStruct((count, columns), BF16),
        ),
        in_specs=[anywhere] * 8,
        out_specs=(anywhere,) * 4,
        scratch_shapes=scratch,
        compiler_params=pltpu.CompilerParams(
            collective_id=0, has_side_effects=True, vmem_limit_bytes=67043328
        ),
        name="layer",
    )(routes, routes.T, route_weight, norm_gain[None], tokens, gate_master, up_master, down_master)


def solution(mesh):
    placed = (
        P("fs", None),
        P("fs", None),
        P("fs", None),
        P("fs"),
        P(None, "fs", "tp"),
        P(None, "fs", "tp"),
        P(None, "fs", "tp"),
    )

    def step(*args):
        gate, up, down, out = body(*args)
        return gate[None], up[None], down[None], out

    return jax.shard_map(
        step,
        mesh=mesh,
        in_specs=placed,
        out_specs=(P("fs", None, "tp"), P("fs", None, "tp"), P("fs", "tp", None), P("fs", "tp")),
        check_vma=False,
    )
```

profile of v0, /device:TPU:16, one launch (start us, length us, event | category | flops | bytes accessed | tf_op | source)
XLA Modules:
  0.0 416.8 jit_solution(10341214358385615674)
XLA Ops:
  0.6 1.6 copy.12.weight_in
  2.3 1.6 copy.11.routes_in
  3.9 401.5 %layer.1 = (bf16[2048,1024]{1,0:T(8,128)(2,1)}, bf16[2048,1024]{1,0:T(8,128)(2,1)}, bf16[1024,2048]{1,0:T(8,128)(2,1)}, bf16[768,512]{1,0:T(8,128)(2,1)}) custom-call(s32[768,2]{1,0:T(8,128)} %copy.11.routes_in, s32[2,768]{1,0:T(2,128)} %bitcast.8, f32[768,2]{1,0:T(8,128)} %copy.12.weight_in, f32[1,256]{1,0:T(1,128)} %bitcast.9, ...), custom_call_target="tpu_custom_call" | custom-call | tf_op jit(solution)/shard_map/layer/pallas_call | solution.py:503
  405.4 0.0 copy-start.1
  405.4 4.8 %copy.17 = bf16[1,2048,1024]{2,1,0:T(8,128)(2,1)} copy(bf16[1,2048,1024]{2,1,0:T(8,128)(2,1)} %bitcast.7) | data formatting | bytes 8388608
  410.2 0.0 copy-done.1
  410.2 0.0 copy-start
  410.2 2.1 copy.18
  412.4 1.6 copy-done
  413.9 0.0 copy-start.2
  413.9 2.0 copy.19
  416.0 0.0 copy-done.2
  416.0 0.9 copy.20
Async XLA Ops:
  405.4 4.8 %copy-start.1 = (bf16[2048,1024]{1,0:T(8,128)(2,1)S(1)}, bf16[2048,1024]{1,0:T(8,128)(2,1)}, u32[]{:S(2)}) copy-start(bf16[2048,1024]{1,0:T(8,128)(2,1)} %get-tuple-element.9) | copy-start | bytes 12582916
  410.2 3.7 copy-start
  413.9 2.0 copy-start.2
where the time goes:
time: 418 us; the launch traced here: 417 us
  Pallas kernels  402 us (96%)
  local copies, waits for them, and re-layouts  14.7 us (4%)
    pallas_call x1, Pallas kernels, body(): pl.pallas_call(functools.partial(kernel, n_fs, n_tp), out_shape=(jax.Shap...  402 us
    unnamed x12, local copies, waits for them, and re-layouts  14.7 us

commit v1 on v0

v1 whole, which is shorter than its diff:
```python
import functools

import jax
import jax.numpy as jnp
from jax import lax
from jax.experimental import pallas as pl
from jax.experimental.pallas import tpu as pltpu
from jax.sharding import PartitionSpec as P

CAP = 216
ROWS = 224
DEPTH = 256
LANES = 128
STAGES = 3
VMEM = 67 * 1000 * 1000
MESH = pl.DeviceIdType.MESH
F32, BF16 = jnp.float32, jnp.bfloat16


def aligned(value, step=LANES):
    return pl.multiple_of(value, step)


def kernel(
    n_fs, n_tp, routes_in, weight_in, gain_in, tokens_in, gate_in, up_in, down_in,
    gate_recv, up_recv, down_recv, result,
    gate_send, up_send, down_send, stage, down_stage,
    tokens, normed, outgoing, incoming, hidden, far, far_recv, near, across_recv,
    back_send, back_recv, gain_row, gain, routes, weight, slot_across, slot, share,
    load_sem, down_load_sem, small_sem, token_load_sem, gate_ss, gate_rs, up_ss, up_rs, token_ss, token_rs,
    down_ss, down_rs, line_ss, line_rs, pair_ss, pair_rs, far_ss, far_rs, across_ss, across_rs,
    back_ss, back_rs,
):
    f, t = lax.axis_index("fs"), lax.axis_index("tp")
    core, x = t % 2, t // 2
    chips = n_tp // 2
    ratio = n_fs // n_tp
    rows, units = gate_send.shape[1:]
    part = down_stage.shape[1]
    columns = down_stage.shape[2]
    chunks = columns // LANES
    half = n_fs // 2

    def remote(src, dst, ss, rs, fs, tp):
        return pltpu.make_async_remote_copy(
            src_ref=src, dst_ref=dst, send_sem=ss, recv_sem=rs,
            device_id={"fs": fs, "tp": tp}, device_id_type=MESH,
        )

    def each(n, action):
        def step(i, carry):
            action(i)
            return carry

        lax.fori_loop(0, n, step, 0)

    def offset(i):
        return jnp.where(i < half, i + half, jnp.where(i == n_fs - 1, 0, i - half + 1))

    small = [
        pltpu.make_async_copy(gain_in, gain_row, small_sem.at[0]),
        pltpu.make_async_copy(routes_in, routes, small_sem.at[1]),
        pltpu.make_async_copy(weight_in, weight, small_sem.at[2]),
    ]
    small[0].start()

    def load(source, i):
        return pltpu.make_async_copy(
            source.at[jnp.bitwise_xor(f, offset(i))], stage.at[i % STAGES], load_sem.at[i % STAGES]
        )

    for i in range(STAGES):
        load(gate_in, i).start()
    for copy in small[1:]:
        copy.start()
    strip = tokens.shape[1]
    count = normed.shape[0]

    def token_load(i):
        return pltpu.make_async_copy(
            tokens_in.at[pl.ds(aligned(i * strip, strip), strip)], tokens.at[i % 2], token_load_sem.at[i % 2]
        )

    token_load(0).start()
    token_load(1).start()

    barrier = pltpu.get_barrier_semaphore()
    total = n_fs * n_tp
    me = f * n_tp + t

    def greet(i):
        other = (me + i + 1) % total
        pl.semaphore_signal(
            barrier, inc=1, device_id={"fs": other // n_tp, "tp": other % n_tp}, device_id_type=MESH
        )

    each(total - 1, greet)

    back_recv[:, :, CAP:, :] = jnp.zeros((chunks, n_fs, DEPTH - CAP, LANES), BF16)

    small[0].wait()
    same = lax.broadcasted_iota(jnp.int32, (rows, rows), 0) == lax.broadcasted_iota(jnp.int32, (rows, rows), 1)
    column = jnp.sum(jnp.where(same, gain_row[...], 0.0), axis=1, keepdims=True)
    gain[...] = jnp.broadcast_to(column, (rows, LANES))

    def weight_copy(send, recv, ss, rs, e, owner):
        return remote(
            send.at[e], recv.at[pl.ds(aligned(owner * rows), rows)], ss.at[e], rs.at[owner], e, t
        )

    def scaled(block):
        scale = gain[...]
        return jnp.concatenate(
            [(block[:, k : k + LANES] * scale).astype(BF16) for k in range(0, units, LANES)], axis=1
        )

    def cast_weights(source, send, recv, sent):
        def step(i):
            e = jnp.bitwise_xor(f, offset(i))
            load(source, i).wait()
            cast = scaled(stage[i % STAGES])

            @pl.when(i < n_fs - 1)
            def _():
                send[e] = cast

            @pl.when(i == n_fs - 1)
            def _():
                recv[pl.ds(aligned(f * rows), rows), :] = cast

            @pl.when(i + STAGES < n_fs)
            def _():
                load(source, i + STAGES).start()

            if sent is not None:
                pl.when(i > 0)(lambda: sent(jnp.bitwise_xor(f, offset(i - 1))))

        each(n_fs, step)

    def send_gate(e):
        weight_copy(gate_send, gate_recv, gate_ss, gate_rs, e, f).start()

    def send_up(e):
        weight_copy(up_send, up_recv, up_ss, up_rs, e, f).start()

    pl.semaphore_wait(barrier, total - 1)
    cast_weights(gate_in, gate_send, gate_recv, send_gate)
    for i in range(STAGES):
        load(up_in, i).start()

    for copy in small[1:3]:
        copy.wait()
    row_id = lax.broadcasted_iota(jnp.int32, (count, count), 0)
    column_id = lax.broadcasted_iota(jnp.int32, (count, count), 1)
    expert_row = lax.broadcasted_iota(jnp.int32, (n_fs, count), 0)
    first, second = expert_row == routes[0:1, :], expert_row == routes[1:2, :]
    named = first | second
    before = jnp.dot(
        jnp.where(named, 1.0, 0.0).astype(BF16),
        jnp.where(row_id < column_id, 1.0, 0.0).astype(BF16),
        preferred_element_type=F32,
    )
    before = jnp.where(named, before, -1.0)
    slot_across[...] = before
    slot[...] = before.T
    share[...] = (jnp.where(first, weight[0:1, :], 0.0) + jnp.where(second, weight[1:2, :], 0.0)).T

    def norm(i):
        at = pl.ds(aligned(i * strip, strip), strip)
        token_load(i).wait()
        values = tokens[i % 2].astype(F32)
        scale = lax.rsqrt(jnp.mean(values * values, axis=1, keepdims=True) + 1e-06)
        mine = tokens[i % 2, :, pl.ds(aligned(t * columns), columns)].astype(F32)
        normed[at, :] = (mine * scale).astype(BF16)

        @pl.when(i + 2 < count // strip)
        def _():
            token_load(i + 2).start()

    each(count // strip, norm)

    def token_copy(e, owner):
        return remote(
            outgoing.at[e, pl.ds(0, CAP)],
            incoming.at[owner, pl.ds(0, CAP), pl.ds(aligned(t * columns), columns)],
            token_ss.at[e],
            token_rs.at[owner],
            e,
            t,
        )

    slot_id = lax.broadcasted_iota(jnp.int32, (ROWS, count), 0).astype(F32)

    def dispatch(i):
        e = jnp.bitwise_xor(f, offset(i))
        pick = jnp.where(slot_id == slot_across[pl.ds(e, 1), :], 1.0, 0.0).astype(BF16)
        picked = jnp.dot(pick, normed[...], preferred_element_type=F32).astype(BF16)

        @pl.when(i < n_fs - 1)
        def _():
            outgoing[e] = picked

        @pl.when(i == n_fs - 1)
        def _():
            incoming[f, :, pl.ds(aligned(t * columns), columns)] = picked

        @pl.when(i > 0)
        def _():
            token_copy(jnp.bitwise_xor(f, offset(i - 1)), f).start()

    each(n_fs, dispatch)

    cast_weights(up_in, up_send, up_recv, None)

    def down_load(i):
        return pltpu.make_async_copy(down_in.at[i], down_stage.at[i % 2], down_load_sem.at[i % 2])

    owner = f // ratio

    def place(c, tp):
        return pl.ds(aligned(tp * columns + c * LANES), LANES)

    def down_copy(c, e, to, fs, tp):
        return remote(
            down_send.at[c, e],
            down_recv.at[pl.ds(aligned(fs % ratio * part), part), place(c, tp)],
            down_ss.at[c, e],
            down_rs.at[c, fs % ratio * n_tp + tp],
            e,
            to,
        )

    down_load(0).start()
    down_load(1).start()

    def down_cast(i):
        down_load(i).wait()
        for c in range(chunks):
            down_send[c, i] = down_stage[i % 2, :, c * LANES : (c + 1) * LANES].astype(BF16)

        @pl.when(i + 2 < n_fs)
        def _():
            down_load(i + 2).start()

    each(n_fs, down_cast)

    def send_down(c):
        def one(i):
            e = jnp.bitwise_xor(f, offset(i))
            mine = (e == f) & (owner == t)

            @pl.when(mine)
            def _():
                down_recv[pl.ds(aligned(f % ratio * part), part), place(c, t)] = down_send[c, e]

            @pl.when(jnp.logical_not(mine))
            def _():
                down_copy(c, e, owner, f, t).start()

        each(n_fs, one)

    def peers(action):
        each(n_fs - 1, lambda i: action(jnp.bitwise_xor(f, i + 1)))

    peers(lambda e: token_copy(e, e).wait_recv())
    each(n_fs - 1, lambda i: send_up(jnp.bitwise_xor(f, offset(i))))

    def span(tp):
        return incoming.at[:, pl.ds(0, CAP), pl.ds(aligned(tp * columns), columns)]

    def line(d, chip):
        other = jnp.bitwise_xor(x, d)
        return remote(
            span(chip * 2 + core), span(chip * 2 + core), line_ss.at[d - 1], line_rs.at[d - 1], f, other * 2 + core
        )

    def pair(d, on):
        chip = jnp.bitwise_xor(x, d)
        return remote(
            span(chip * 2 + on), span(chip * 2 + on), pair_ss.at[d], pair_rs.at[d], f, x * 2 + 1 - core
        )

    for d in range(1, chips):
        line(d, x).start()
    pair(0, core).start()
    for d in range(1, chips):
        line(d, jnp.bitwise_xor(x, d)).wait_recv()
        pair(d, core).start()
    for d in range(chips):
        pair(d, 1 - core).wait_recv()

    peers(lambda e: weight_copy(gate_send, gate_recv, gate_ss, gate_rs, e, e).wait_recv())
    peers(lambda e: weight_copy(up_send, up_recv, up_ss, up_rs, e, e).wait_recv())
    each(chunks, send_down)
    tile = 256
    width = incoming.shape[2]
    group = 2

    def hidden_step(i):
        g, n = i // (units // tile), i % (units // tile)
        lanes = pl.ds(aligned(n * tile, tile), tile)
        at = pl.ds(g * group, group)
        received = incoming[at].reshape(group * ROWS, width)
        gate_pre = jnp.dot(received, gate_recv[:, lanes], preferred_element_type=F32)
        up_pre = jnp.dot(received, up_recv[:, lanes], preferred_element_type=F32)
        value = gate_pre / (1.0 + jnp.exp(-gate_pre)) * up_pre
        hidden[at, :, lanes] = value.astype(BF16).reshape(group, ROWS, tile)

    each(n_fs // group * (units // tile), hidden_step)

    def far_copy(c):
        return remote(far, far_recv.at[c], far_ss.at[c], far_rs.at[c], f, x * 2 + 1 - core)

    def across_copy(c, d):
        other = jnp.bitwise_xor(x, d)
        return remote(
            near.at[c % 2, other], across_recv.at[c, d - 1], across_ss.at[c, d - 1], across_rs.at[c, d - 1],
            f, other * 2 + core,
        )

    def back_copy(c, e, owner):
        return remote(
            back_send.at[c, e, pl.ds(0, CAP)],
            back_recv.at[c, owner, pl.ds(0, CAP)],
            back_ss.at[c, e],
            back_rs.at[c, owner],
            e,
            t,
        )

    def send_back(c):
        peers(lambda e: back_copy(c, e, f).start())

    def product(c, side, store):
        taken = jnp.concatenate([down_recv[:, place(c, 2 * chip + side)] for chip in range(chips)], axis=1)

        def step(g):
            at = pl.ds(g * group, group)
            value = jnp.dot(
                hidden[at].reshape(group * ROWS, units), taken, preferred_element_type=F32
            ).astype(BF16)
            for chip in range(chips):
                store(chip, at, value[:, chip * LANES : (chip + 1) * LANES].reshape(group, ROWS, LANES))

        each(n_fs // group, step)

    def store_far(chip, at, value):
        far[chip, at] = value

    def finish(c):
        for d in range(1, chips):
            across_copy(c, d).wait_recv()

        def one(e):
            value = near[c % 2, x, e].astype(F32) + far_recv[c, x, e].astype(F32)
            for d in range(1, chips):
                value = value + across_recv[c, d - 1, e].astype(F32)
            back_send[c, e] = value.astype(BF16)

        each(n_fs, one)
        back_recv[c, f, pl.ds(0, CAP), :] = back_send[c, f, pl.ds(0, CAP), :]

    def down_chunk(c):
        def store_near(chip, at, value):
            near[c % 2, chip, at] = value

        def arrival(i):
            fs, tp = t * ratio + i // n_tp, i % n_tp

            @pl.when(jnp.logical_not((fs == f) & (tp == t)))
            def _():
                down_copy(c, f, t, fs, tp).wait_recv()

        each(ratio * n_tp, arrival)

        @pl.when(c == chunks - 1)
        def _():
            each(chunks - 2, send_back)

        product(c, 1 - core, store_far)
        far_copy(c).start()

        @pl.when(c > 1)
        def _():
            for d in range(1, chips):
                across_copy(c - 2, d).wait_send()

        product(c, core, store_near)
        far_copy(c).wait()
        for d in range(1, chips):
            other = jnp.bitwise_xor(x, d)

            def add(e):
                total = near[c % 2, other, e].astype(F32) + far_recv[c, other, e].astype(F32)
                near[c % 2, other, e] = total.astype(BF16)

            each(n_fs, add)
            across_copy(c, d).start()

        @pl.when(c > 0)
        def _():
            finish(c - 1)

    each(chunks, down_chunk)
    send_back(chunks - 2)
    finish(chunks - 1)
    send_back(chunks - 1)
    for c in range(chunks - 2, chunks):
        for d in range(1, chips):
            across_copy(c, d).wait_send()

    lane_id = lax.broadcasted_iota(jnp.int32, (count, DEPTH), 1).astype(F32)

    def combine(c):
        peers(lambda e: back_copy(c, e, e).wait_recv())
        value = jnp.zeros((count, LANES), F32)
        for e in range(n_fs):
            pick = jnp.where(lane_id == slot[:, e : e + 1], 1.0, 0.0).astype(BF16)
            value = value + share[:, e : e + 1] * jnp.dot(pick, back_recv[c, e], preferred_element_type=F32)
        result[:, pl.ds(aligned(c * LANES), LANES)] = value.astype(BF16)

    each(chunks, combine)

    peers(lambda e: weight_copy(gate_send, gate_recv, gate_ss, gate_rs, e, f).wait_send())
    peers(lambda e: weight_copy(up_send, up_recv, up_ss, up_rs, e, f).wait_send())
    peers(lambda e: token_copy(e, f).wait_send())
    for d in range(1, chips):
        line(d, x).wait_send()
    for d in range(chips):
        pair(d, core).wait_send()

    def drain(c):
        def one(e):
            @pl.when(jnp.logical_not((e == f) & (owner == t)))
            def _():
                down_copy(c, e, owner, f, t).wait_send()

        each(n_fs, one)
        peers(lambda e: back_copy(c, e, f).wait_send())

    each(chunks, drain)


def body(tokens, routes, route_weight, norm_gain, gate_master, up_master, down_master):
    n_fs, n_tp = lax.axis_size("fs"), lax.axis_size("tp")
    count, width = tokens.shape
    experts, rows, units = gate_master.shape
    part, columns = down_master.shape[1:]
    chips, chunks, ratio = n_tp // 2, columns // LANES, n_fs // n_tp
    assert experts == n_fs
    dma = pltpu.SemaphoreType.DMA
    lines = max(1, chips - 1)
    scratch = [
        pltpu.VMEM((n_fs, rows, units), BF16),
        pltpu.VMEM((n_fs, rows, units), BF16),
        pltpu.VMEM((chunks, n_fs, part, LANES), BF16),
        pltpu.VMEM((STAGES, rows, units), F32),
        pltpu.VMEM((2, part, columns), F32),
        pltpu.VMEM((2, count // 8, width), BF16),
        pltpu.VMEM((count, columns), BF16),
        pltpu.VMEM((n_fs, ROWS, columns), BF16),
        pltpu.VMEM((n_fs, ROWS, width), BF16),
        pltpu.VMEM((n_fs, ROWS, units), BF16),
        pltpu.VMEM((chips, n_fs, ROWS, LANES), BF16),
        pltpu.VMEM((chunks, chips, n_fs, ROWS, LANES), BF16),
        pltpu.VMEM((2, chips, n_fs, ROWS, LANES), BF16),
        pltpu.VMEM((chunks, lines, n_fs, ROWS, LANES), BF16),
        pltpu.VMEM((chunks, n_fs, ROWS, LANES), BF16),
        pltpu.VMEM((chunks, n_fs, DEPTH, LANES), BF16),
        pltpu.VMEM((1, rows), F32),
        pltpu.VMEM((rows, LANES), F32),
        pltpu.VMEM((2, count), jnp.int32),
        pltpu.VMEM((2, count), F32),
        pltpu.VMEM((n_fs, count), F32),
        pltpu.VMEM((count, n_fs), F32),
        pltpu.VMEM((count, n_fs), F32),
        dma((STAGES,)), dma((2,)), dma((3,)), dma((2,)),
        dma((n_fs,)), dma((n_fs,)), dma((n_fs,)), dma((n_fs,)), dma((n_fs,)), dma((n_fs,)),
        dma((chunks, n_fs)), dma((chunks, ratio * n_tp)),
        dma((lines,)), dma((lines,)), dma((chips,)), dma((chips,)),
        dma((chunks,)), dma((chunks,)), dma((chunks, lines)), dma((chunks, lines)),
        dma((chunks, n_fs)), dma((chunks, n_fs)),
    ]
    shapes = (
        (n_fs * rows, units), (n_fs * rows, units), (ratio * part, n_tp * columns), (count, columns)
    )
    kept = sum(2 * a * b for a, b in shapes)
    anywhere = pl.BlockSpec(memory_space=pl.ANY)
    return pl.pallas_call(
        functools.partial(kernel, n_fs, n_tp),
        out_shape=tuple(pltpu.VMEM(shape, BF16) for shape in shapes),
        in_specs=[anywhere] * 7,
        out_specs=(pl.BlockSpec(memory_space=pltpu.VMEM),) * 4,
        scratch_shapes=scratch,
        compiler_params=pltpu.CompilerParams(
            collective_id=0, has_side_effects=True, vmem_limit_bytes=VMEM - kept
        ),
        name="layer",
    )(routes.T, route_weight.T, norm_gain[None], tokens, gate_master, up_master, down_master)


def solution(mesh):
    placed = (
        P("fs", None),
        P("fs", None),
        P("fs", None),
        P("fs"),
        P(None, "fs", "tp"),
        P(None, "fs", "tp"),
        P(None, "fs", "tp"),
    )

    def step(*args):
        gate, up, down, out = body(*args)
        return gate[None], up[None], down[None], out

    return jax.shard_map(
        step,
        mesh=mesh,
        in_specs=placed,
        out_specs=(P("fs", None, "tp"), P("fs", None, "tp"), P("fs", "tp", None), P("fs", "tp")),
        check_vma=False,
    )
```

time: 418 us -> 371 us (0.89)
  Pallas kernels: 402 us -> 361 us
  local copies, waits for them, and re-layouts: 14.7 us -> 6.92 us
    pallas_call x1, Pallas kernels: 402 us -> 361 us  [body(): pl.pallas_call(functools.partial(kernel, n_fs, n_tp), out_shape=tuple((pl...]
    unnamed x12 -> x4, local copies, waits for them, and re-layouts: 14.7 us -> 6.92 us
where the time goes in v1:
time: 371 us; the launch traced here: 368 us
  Pallas kernels  361 us (97%)
  local copies, waits for them, and re-layouts  6.92 us (2%)
    pallas_call x1, Pallas kernels, body(): pl.pallas_call(functools.partial(kernel, n_fs, n_tp), out_shape=tuple((pl...  361 us

profile of v1, /device:TPU:16, one launch (start us, length us, event | category | flops | bytes accessed | tf_op | source)
XLA Modules:
  0.0 368.2 jit_solution(1212345976323200195)
XLA Ops:
  0.6 360.6 %layer.1 = (bf16[2048,1024]{1,0:T(8,128)(2,1)S(1)}, bf16[2048,1024]{1,0:T(8,128)(2,1)S(1)}, bf16[1024,2048]{1,0:T(8,128)(2,1)S(1)}, bf16[768,512]{1,0:T(8,128)(2,1)S(1)}) custom-call(s32[2,768]{1,0:T(2,128)} %bitcast.9, f32[2,768]{1,0:T(2,128)} %bitcast.10, f32[1,256]{1,0:T(1,128)} %bitcast.11, bf16[768,2048]{1,0:T(8,128)(2,1)} %tokens_in.1, ...), custom_call_target="tpu_custom_call" | custom-call | tf_op jit(solution)/shard_map/layer/pallas_call | solution.py:489
  361.3 2.0 copy.15
  363.3 2.0 copy.16
  365.3 0.9 copy.18
  366.2 2.0 copy.17

commit v2 on v1

--- a/solution.py
+++ b/solution.py
@@ -21,12 +21,40 @@
     return pl.multiple_of(value, step)
 
 
+def weighted(slot, share, rows_of):
+    count, n_fs = slot.shape
+    lane_id = lax.broadcasted_iota(jnp.int32, (count, DEPTH), 1).astype(F32)
+    value = jnp.zeros((count, LANES), F32)
+    for e in range(n_fs):
+        pick = jnp.where(lane_id == slot[:, e : e + 1], 1.0, 0.0).astype(BF16)
+        value = value + share[:, e : e + 1] * jnp.dot(pick, rows_of(e), preferred_element_type=F32)
+    return value.astype(BF16)
+
+
+def store_kernel(gate, up, down, result, back, slot, share, gate_out, up_out, down_out, layer_out, last, sem):
+    early = result.shape[1] - LANES
+    copies = [
+        pltpu.make_async_copy(gate, gate_out, sem.at[0]),
+        pltpu.make_async_copy(up, up_out, sem.at[1]),
+        pltpu.make_async_copy(down, down_out, sem.at[2]),
+        pltpu.make_async_copy(result.at[:, pl.ds(0, early)], layer_out.at[:, pl.ds(0, early)], sem.at[3]),
+    ]
+    for copy in copies:
+        copy.start()
+    chunk = back.shape[0] - 1
+    last[...] = weighted(slot, share, lambda e: back[chunk, e])
+    copies.append(pltpu.make_async_copy(last, layer_out.at[:, pl.ds(early, LANES)], sem.at[4]))
+    copies[-1].start()
+    for copy in copies:
+        copy.wait()
+
+
 def kernel(
     n_fs, n_tp, routes_in, weight_in, gain_in, tokens_in, gate_in, up_in, down_in,
-    gate_recv, up_recv, down_recv, result,
+    gate_recv, up_recv, down_recv, result, back_recv, slot, share,
     gate_send, up_send, down_send, stage, down_stage,
     tokens, normed, outgoing, incoming, hidden, far, far_recv, near, across_recv,
-    back_send, back_recv, gain_row, gain, routes, weight, slot_across, slot, share,
+    back_send, gain_row, gain, routes, weight, slot_across,
     load_sem, down_load_sem, small_sem, token_load_sem, gate_ss, gate_rs, up_ss, up_rs, token_ss, token_rs,
     down_ss, down_rs, line_ss, line_rs, pair_ss, pair_rs, far_ss, far_rs, across_ss, across_rs,
     back_ss, back_rs,
@@ -132,10 +160,17 @@
             def _():
                 load(source, i + STAGES).start()
 
-            if sent is not None:
-                pl.when(i > 0)(lambda: sent(jnp.bitwise_xor(f, offset(i - 1))))
-
-        each(n_fs, step)
+        def send_step(i):
+            step(i)
+            sent(jnp.bitwise_xor(f, offset(i - 1)))
+
+        if sent is None:
+            each(n_fs, step)
+        else:
+            each(2, step)
+            pl.semaphore_wait(barrier, total - 1)
+            sent(jnp.bitwise_xor(f, offset(0)))
+            each(n_fs - 2, lambda i: send_step(i + 2))
 
     def send_gate(e):
         weight_copy(gate_send, gate_recv, gate_ss, gate_rs, e, f).start()
@@ -143,7 +178,6 @@
     def send_up(e):
         weight_copy(up_send, up_recv, up_ss, up_rs, e, f).start()
 
-    pl.semaphore_wait(barrier, total - 1)
     cast_weights(gate_in, gate_send, gate_recv, send_gate)
     for i in range(STAGES):
         load(up_in, i).start()
@@ -409,17 +443,12 @@
         for d in range(1, chips):
             across_copy(c, d).wait_send()
 
-    lane_id = lax.broadcasted_iota(jnp.int32, (count, DEPTH), 1).astype(F32)
-
     def combine(c):
         peers(lambda e: back_copy(c, e, e).wait_recv())
-        value = jnp.zeros((count, LANES), F32)
-        for e in range(n_fs):
-            pick = jnp.where(lane_id == slot[:, e : e + 1], 1.0, 0.0).astype(BF16)
-            value = value + share[:, e : e + 1] * jnp.dot(pick, back_recv[c, e], preferred_element_type=F32)
-        result[:, pl.ds(aligned(c * LANES), LANES)] = value.astype(BF16)
-
-    each(chunks, combine)
+        result[:, pl.ds(aligned(c * LANES), LANES)] = weighted(slot, share, lambda e: back_recv[c, e])
+
+    each(chunks - 1, combine)
+    peers(lambda e: back_copy(chunks - 1, e, e).wait_recv())
 
     peers(lambda e: weight_copy(gate_send, gate_recv, gate_ss, gate_rs, e, f).wait_send())
     peers(lambda e: weight_copy(up_send, up_recv, up_ss, up_rs, e, f).wait_send())
@@ -466,14 +495,11 @@
         pltpu.VMEM((2, chips, n_fs, ROWS, LANES), BF16),
         pltpu.VMEM((chunks, lines, n_fs, ROWS, LANES), BF16),
         pltpu.VMEM((chunks, n_fs, ROWS, LANES), BF16),
-        pltpu.VMEM((chunks, n_fs, DEPTH, LANES), BF16),
         pltpu.VMEM((1, rows), F32),
         pltpu.VMEM((rows, LANES), F32),
         pltpu.VMEM((2, count), jnp.int32),
         pltpu.VMEM((2, count), F32),
         pltpu.VMEM((n_fs, count), F32),
-        pltpu.VMEM((count, n_fs), F32),
-        pltpu.VMEM((count, n_fs), F32),
         dma((STAGES,)), dma((2,)), dma((3,)), dma((2,)),
         dma((n_fs,)), dma((n_fs,)), dma((n_fs,)), dma((n_fs,)), dma((n_fs,)), dma((n_fs,)),
         dma((chunks, n_fs)), dma((chunks, ratio * n_tp)),
@@ -484,19 +510,33 @@
     shapes = (
         (n_fs * rows, units), (n_fs * rows, units), (ratio * part, n_tp * columns), (count, columns)
     )
-    kept = sum(2 * a * b for a, b in shapes)
-    anywhere = pl.BlockSpec(memory_space=pl.ANY)
-    return pl.pallas_call(
+    kept = sum(2 * a * b for a, b in shapes) + 2 * chunks * n_fs * DEPTH * LANES + 8 * count * LANES
+    anywhere, vector = pl.BlockSpec(memory_space=pl.ANY), pl.BlockSpec(memory_space=pltpu.VMEM)
+    held = pl.pallas_call(
         functools.partial(kernel, n_fs, n_tp),
-        out_shape=tuple(pltpu.VMEM(shape, BF16) for shape in shapes),
+        out_shape=(
+            *(pltpu.VMEM(shape, BF16) for shape in shapes),
+            pltpu.VMEM((chunks, n_fs, DEPTH, LANES), BF16),
+            pltpu.VMEM((count, n_fs), F32),
+            pltpu.VMEM((count, n_fs), F32),
+        ),
         in_specs=[anywhere] * 7,
-        out_specs=(pl.BlockSpec(memory_space=pltpu.VMEM),) * 4,
+        out_specs=(vector,) * 7,
         scratch_shapes=scratch,
         compiler_params=pltpu.CompilerParams(
             collective_id=0, has_side_effects=True, vmem_limit_bytes=VMEM - kept
         ),
         name="layer",
     )(routes.T, route_weight.T, norm_gain[None], tokens, gate_master, up_master, down_master)
+    return pl.pallas_call(
+        store_kernel,
+        out_shape=tuple(jax.ShapeDtypeStruct(shape, BF16) for shape in shapes),
+        in_specs=[vector] * 7,
+        out_specs=(anywhere,) * 4,
+        scratch_shapes=[pltpu.VMEM((count, LANES), BF16), dma((5,))],
+        compiler_params=pltpu.CompilerParams(vmem_limit_bytes=16 * 1000 * 1000),
+        name="store",
+    )(*(pltpu.with_memory_space_constraint(value, pltpu.VMEM) for value in held))
 
 
 def solution(mesh):

time: 371 us -> 367 us (0.989)
  local copies, waits for them, and re-layouts: 6.92 us -> 0 us
  Pallas kernels: 361 us -> 365 us
    unnamed x4 -> x0, local copies, waits for them, and re-layouts: 6.92 us -> none
    pallas_call x1 -> x2, Pallas kernels: 361 us -> 365 us  [the longest x1 360 us: body(): pl.pallas_call(functools.partial(kernel, n_fs, n_tp), out_shape=(*(pltpu....]
where the time goes in v2:
time: 367 us; the launch traced here: 365 us
  Pallas kernels  365 us (99%)
    pallas_call x1, Pallas kernels, body(): pl.pallas_call(functools.partial(kernel, n_fs, n_tp), out_shape=(*(pltpu....  360 us

profile of v2, /device:TPU:16, one launch (start us, length us, event | category | flops | bytes accessed | tf_op | source)
XLA Modules:
  0.0 365.2 jit_solution(13742900119668018218)
XLA Ops:
  0.6 359.7 %layer.1 = (bf16[2048,1024]{1,0:T(8,128)(2,1)S(1)}, bf16[2048,1024]{1,0:T(8,128)(2,1)S(1)}, bf16[1024,2048]{1,0:T(8,128)(2,1)S(1)}, bf16[768,512]{1,0:T(8,128)(2...) custom-call(s32[2,768]{1,0:T(2,128)} %bitcast.6, f32[2,768]{1,0:T(2,128)} %bitcast.7, ...), custom_call_target="tpu_custom_call" | custom-call | tf_op jit(solution)/shard_map/layer/pallas_call | solution.py:515
  360.3 4.8 %store.1 = (bf16[2048,1024]{1,0:T(8,128)(2,1)}, bf16[2048,1024]{1,0:T(8,128)(2,1)}, bf16[1024,2048]{1,0:T(8,128)(2,1)}, bf16[768,512]{1,0:T(8,128)(2,1)}) custom-call(bf16[2048,1024]{1,0:T(8,128)(2,1)S(1)} %get-tuple-element.15.gate, bf16[2048,1024]{1,0:T(8,128)(2,1)S(1)} %get-tuple-element.16.up, bf16[1024,2048]{1,0:T(8,128)(2,1)S(1)} %get-tuple-element.17.down, ...), custom_call_target="tpu_custom_call" | custom-call | tf_op jit(solution)/shard_map/store/pallas_call | solution.py:531

commit v3 on v2

--- a/solution.py
+++ b/solution.py
@@ -298,6 +298,7 @@
 
     peers(lambda e: token_copy(e, e).wait_recv())
     each(n_fs - 1, lambda i: send_up(jnp.bitwise_xor(f, offset(i))))
+    send_down(0)
 
     def span(tp):
         return incoming.at[:, pl.ds(0, CAP), pl.ds(aligned(tp * columns), columns)]
@@ -325,7 +326,7 @@
 
     peers(lambda e: weight_copy(gate_send, gate_recv, gate_ss, gate_rs, e, e).wait_recv())
     peers(lambda e: weight_copy(up_send, up_recv, up_ss, up_rs, e, e).wait_recv())
-    each(chunks, send_down)
+    each(chunks - 1, lambda c: send_down(c + 1))
     tile = 256
     width = incoming.shape[2]
     group = 2
@@ -407,9 +408,6 @@
 
         each(ratio * n_tp, arrival)
 
-        @pl.when(c == chunks - 1)
-        def _():
-            each(chunks - 2, send_back)
 
         product(c, 1 - core, store_far)
         far_copy(c).start()
@@ -434,9 +432,9 @@
         @pl.when(c > 0)
         def _():
             finish(c - 1)
+            send_back(c - 1)
 
     each(chunks, down_chunk)
-    send_back(chunks - 2)
     finish(chunks - 1)
     send_back(chunks - 1)
     for c in range(chunks - 2, chunks):

time: 367 us -> 365 us (level)
  no operation moved by 1% of the time
where the time goes in v3:
time: 365 us
  Pallas kernels  364 us (100%)
    pallas_call x1, Pallas kernels, body(): pl.pallas_call(functools.partial(kernel, n_fs, n_tp), out_shape=(*(pltpu....  359 us

profile of v3, /device:TPU:16, one launch (start us, length us, event | category | flops | bytes accessed | tf_op | source)
XLA Modules:
  0.0 364.8 jit_solution(17305097179611435792)
XLA Ops:
  0.6 359.4 %layer.1 = (bf16[2048,1024]{1,0:T(8,128)(2,1)S(1)}, bf16[2048,1024]{1,0:T(8,128)(2,1)S(1)}, bf16[1024,2048]{1,0:T(8,128)(2,1)S(1)}, bf16[768,512]{1,0:T(8,128)(2...) custom-call(s32[2,768]{1,0:T(2,128)} %bitcast.6, f32[2,768]{1,0:T(2,128)} %bitcast.7, ...), custom_call_target="tpu_custom_call" | custom-call | tf_op jit(solution)/shard_map/layer/pallas_call | solution.py:513
  360.0 4.8 %store.1 = (bf16[2048,1024]{1,0:T(8,128)(2,1)}, bf16[2048,1024]{1,0:T(8,128)(2,1)}, bf16[1024,2048]{1,0:T(8,128)(2,1)}, bf16[768,512]{1,0:T(8,128)(2,1)}) custom-call(bf16[2048,1024]{1,0:T(8,128)(2,1)S(1)} %get-tuple-element.15.gate, bf16[2048,1024]{1,0:T(8,128)(2,1)S(1)} %get-tuple-element.16.up, bf16[1024,2048]{1,0:T(8,128)(2,1)S(1)} %get-tuple-element.17.down, ...), custom_call_target="tpu_custom_call" | custom-call | tf_op jit(solution)/shard_map/store/pallas_call | solution.py:529

commit v4 on v3

--- a/solution.py
+++ b/solution.py
@@ -343,13 +343,23 @@
 
     each(n_fs // group * (units // tile), hidden_step)
 
-    def far_copy(c):
-        return remote(far, far_recv.at[c], far_ss.at[c], far_rs.at[c], f, x * 2 + 1 - core)
-
-    def across_copy(c, d):
+    def first(part_id):
+        return jnp.bitwise_xor(f // half, 1 - part_id) * half
+
+    def senders(part_id):
+        return pl.ds(first(part_id), half)
+
+    def far_copy(c, part_id):
+        return remote(
+            far.at[:, senders(part_id)], far_recv.at[c, :, senders(part_id)],
+            far_ss.at[c, part_id], far_rs.at[c, part_id], f, x * 2 + 1 - core,
+        )
+
+    def across_copy(c, d, part_id):
         other = jnp.bitwise_xor(x, d)
         return remote(
-            near.at[c % 2, other], across_recv.at[c, d - 1], across_ss.at[c, d - 1], across_rs.at[c, d - 1],
+            near.at[c % 2, other, senders(part_id)], across_recv.at[c, d - 1, senders(part_id)],
+            across_ss.at[c, 2 * (d - 1) + part_id], across_rs.at[c, 2 * (d - 1) + part_id],
             f, other * 2 + core,
         )
 
@@ -363,36 +373,42 @@
             t,
         )
 
-    def send_back(c):
-        peers(lambda e: back_copy(c, e, f).start())
-
-    def product(c, side, store):
+    def send_back(c, part_id):
+        if part_id == 0:
+            each(half, lambda i: back_copy(c, jnp.bitwise_xor(f, half + i), f).start())
+        else:
+            each(half - 1, lambda i: back_copy(c, jnp.bitwise_xor(f, i + 1), f).start())
+
+    def product(c, side, part_id, store):
         taken = jnp.concatenate([down_recv[:, place(c, 2 * chip + side)] for chip in range(chips)], axis=1)
 
         def step(g):
-            at = pl.ds(g * group, group)
+            at = pl.ds(first(part_id) + g * group, group)
             value = jnp.dot(
                 hidden[at].reshape(group * ROWS, units), taken, preferred_element_type=F32
             ).astype(BF16)
             for chip in range(chips):
                 store(chip, at, value[:, chip * LANES : (chip + 1) * LANES].reshape(group, ROWS, LANES))
 
-        each(n_fs // group, step)
+        each(half // group, step)
 
     def store_far(chip, at, value):
         far[chip, at] = value
 
     def finish(c):
-        for d in range(1, chips):
-            across_copy(c, d).wait_recv()
-
-        def one(e):
-            value = near[c % 2, x, e].astype(F32) + far_recv[c, x, e].astype(F32)
+        for part_id in range(2):
             for d in range(1, chips):
-                value = value + across_recv[c, d - 1, e].astype(F32)
-            back_send[c, e] = value.astype(BF16)
-
-        each(n_fs, one)
+                across_copy(c, d, part_id).wait_recv()
+
+            def one(i):
+                e = first(part_id) + i
+                value = near[c % 2, x, e].astype(F32) + far_recv[c, x, e].astype(F32)
+                for d in range(1, chips):
+                    value = value + across_recv[c, d - 1, e].astype(F32)
+                back_send[c, e] = value.astype(BF16)
+
+            each(half, one)
+            send_back(c, part_id)
         back_recv[c, f, pl.ds(0, CAP), :] = back_send[c, f, pl.ds(0, CAP), :]
 
     def down_chunk(c):
@@ -409,44 +425,45 @@
         each(ratio * n_tp, arrival)
 
 
-        product(c, 1 - core, store_far)
-        far_copy(c).start()
-
         @pl.when(c > 1)
         def _():
+            wait_across(c - 2)
+
+        for part_id in range(2):
+            product(c, 1 - core, part_id, store_far)
+            far_copy(c, part_id).start()
+            product(c, core, part_id, store_near)
+            far_copy(c, part_id).wait()
             for d in range(1, chips):
-                across_copy(c - 2, d).wait_send()
-
-        product(c, core, store_near)
-        far_copy(c).wait()
-        for d in range(1, chips):
-            other = jnp.bitwise_xor(x, d)
-
-            def add(e):
-                total = near[c % 2, other, e].astype(F32) + far_recv[c, other, e].astype(F32)
-                near[c % 2, other, e] = total.astype(BF16)
-
-            each(n_fs, add)
-            across_copy(c, d).start()
+                other = jnp.bitwise_xor(x, d)
+
+                def add(i):
+                    e = first(part_id) + i
+                    value = near[c % 2, other, e].astype(F32) + far_recv[c, other, e].astype(F32)
+                    near[c % 2, other, e] = value.astype(BF16)
+
+                each(half, add)
+                across_copy(c, d, part_id).start()
 
         @pl.when(c > 0)
         def _():
             finish(c - 1)
-            send_back(c - 1)
+
+    def wait_across(c):
+        for part_id in range(2):
+            for d in range(1, chips):
+                across_copy(c, d, part_id).wait_send()
 
     each(chunks, down_chunk)
     finish(chunks - 1)
-    send_back(chunks - 1)
     for c in range(chunks - 2, chunks):
-        for d in range(1, chips):
-            across_copy(c, d).wait_send()
+        wait_across(c)
 
     def combine(c):
         peers(lambda e: back_copy(c, e, e).wait_recv())
         result[:, pl.ds(aligned(c * LANES), LANES)] = weighted(slot, share, lambda e: back_recv[c, e])
 
     each(chunks - 1, combine)
-    peers(lambda e: back_copy(chunks - 1, e, e).wait_recv())
 
     peers(lambda e: weight_copy(gate_send, gate_recv, gate_ss, gate_rs, e, f).wait_send())
     peers(lambda e: weight_copy(up_send, up_recv, up_ss, up_rs, e, f).wait_send())
@@ -463,9 +480,10 @@
                 down_copy(c, e, owner, f, t).wait_send()
 
         each(n_fs, one)
-        peers(lambda e: back_copy(c, e, f).wait_send())
 
     each(chunks, drain)
+    each(chunks, lambda c: peers(lambda e: back_copy(c, e, f).wait_send()))
+    peers(lambda e: back_copy(chunks - 1, e, e).wait_recv())
 
 
 def body(tokens, routes, route_weight, norm_gain, gate_master, up_master, down_master):
@@ -502,7 +520,7 @@
         dma((n_fs,)), dma((n_fs,)), dma((n_fs,)), dma((n_fs,)), dma((n_fs,)), dma((n_fs,)),
         dma((chunks, n_fs)), dma((chunks, ratio * n_tp)),
         dma((lines,)), dma((lines,)), dma((chips,)), dma((chips,)),
-        dma((chunks,)), dma((chunks,)), dma((chunks, lines)), dma((chunks, lines)),
+        dma((chunks, 2)), dma((chunks, 2)), dma((chunks, 2 * lines)), dma((chunks, 2 * lines)),
         dma((chunks, n_fs)), dma((chunks, n_fs)),
     ]
     shapes = (

time: 365 us -> 364 us (level)
  no operation moved by 1% of the time
where the time goes in v4:
time: 364 us
  Pallas kernels  363 us (100%)
    pallas_call x1, Pallas kernels, body(): pl.pallas_call(functools.partial(kernel, n_fs, n_tp), out_shape=(*(pltpu....  358 us

profile of v4, /device:TPU:16, one launch (start us, length us, event | category | flops | bytes accessed | tf_op | source)
XLA Modules:
  0.0 363.9 jit_solution(7305564225584495240)
XLA Ops:
  0.6 358.5 %layer.1 = (bf16[2048,1024]{1,0:T(8,128)(2,1)S(1)}, bf16[2048,1024]{1,0:T(8,128)(2,1)S(1)}, bf16[1024,2048]{1,0:T(8,128)(2,1)S(1)}, bf16[768,512]{1,0:T(8,128)(2...) custom-call(s32[2,768]{1,0:T(2,128)} %bitcast.6, f32[2,768]{1,0:T(2,128)} %bitcast.7, ...), custom_call_target="tpu_custom_call" | custom-call | tf_op jit(solution)/shard_map/layer/pallas_call | solution.py:531
  359.1 4.8 %store.1 = (bf16[2048,1024]{1,0:T(8,128)(2,1)}, bf16[2048,1024]{1,0:T(8,128)(2,1)}, bf16[1024,2048]{1,0:T(8,128)(2,1)}, bf16[768,512]{1,0:T(8,128)(2,1)}) custom-call(bf16[2048,1024]{1,0:T(8,128)(2,1)S(1)} %get-tuple-element.15.gate, bf16[2048,1024]{1,0:T(8,128)(2,1)S(1)} %get-tuple-element.16.up, bf16[1024,2048]{1,0:T(8,128)(2,1)S(1)} %get-tuple-element.17.down, ...), custom_call_target="tpu_custom_call" | custom-call | tf_op jit(solution)/shard_map/store/pallas_call | solution.py:547
